TPU v7x, 32 devices: a whole 2x2x4 slice. The times are simulated.
32 devices in a mesh: sp: 8 (over z, x), tp: 4 (over y, core).
Axes of the slice: x: 2, y: 2, z: 4, core: 2. Of those that a mesh axis runs over, the one named last changes fastest.
Arguments:
- latent: bfloat16 [4096, 2048], P(('sp', 'tp')), may hold values from -6 to 6
- context: bfloat16 [512, 2048], P('sp'), may hold values from -6 to 6
- conditioning: float32 [2048], P('sp'), may hold values from -6 to 6
- context_conditioning: float32 [2048], P('sp'), may hold values from -6 to 6
- shift_weight: bfloat16 [2048, 2048], P('sp', 'tp'), may hold values from -0.25 to 0.25
- scale_weight: bfloat16 [2048, 2048], P('sp', 'tp'), may hold values from -0.25 to 0.25
- gate_weight: bfloat16 [2048, 2048], P('sp', 'tp'), may hold values from -0.25 to 0.25
- norm_gain: float32 [2048], replicated, may hold values from 0.1 to 1.9
- query_weight: bfloat16 [2048, 2048], P(None, 'tp'), may hold values from -0.125 to 0.125
- key_weight: bfloat16 [2048, 1024], P(None, 'tp'), may hold values from -0.125 to 0.125
- value_weight: bfloat16 [2048, 1024], P(None, 'tp'), may hold values from -0.125 to 0.125
- query_gain: float32 [64], replicated, may hold values from 2 to 64, as said below
- key_gain: float32 [64], replicated, may hold values from 0.1 to 1.9
- context_lift: float32 [32], P('tp'), may hold values from 1.5 to 3
- output_weight: bfloat16 [2048, 2048], P('tp'), may hold values from -0.125 to 0.125
Outputs:
- mixed: bfloat16 [4096, 2048], P(('sp', 'tp'))
Inputs may be any that keep to these rules, and one draw needn't show every extreme that they name: `query_gain`: one gain for each channel of a head.
All inputs are finite; a program needn't handle non-finite values.
Results may differ from a plain program's by a relative error of at most 0.018.
The roundings to bfloat16 on the way count: a program that leaves them out, or rounds other values in their place, can miss the bound.
Values may be sent and summed in bfloat16 or wider, within the bound.
A program may use at most 128 MiB of HBM per device.

v0:
```python
import math
import jax
import jax.numpy as jnp
from jax import lax
from jax.sharding import PartitionSpec as P

HEAD = 64
GRID = 64
EPSILON = 1e-06
ROTARY_BASE = 10000.0


def normalize(values, gain):
    return values * lax.rsqrt(jnp.mean(values * values, axis=-1, keepdims=True) + EPSILON) * gain


def rotary_tables(offset, count):
    position = offset + jnp.arange(count, dtype=jnp.int32)
    grid_row = (position // GRID).astype(jnp.float32)
    grid_column = (position % GRID).astype(jnp.float32)
    quarter = HEAD // 4
    frequency = ROTARY_BASE ** (-jnp.arange(quarter, dtype=jnp.float32) / quarter)
    angles = jnp.concatenate(
        [grid_row[:, None] * frequency, grid_column[:, None] * frequency], axis=1
    )
    return (jnp.repeat(jnp.cos(angles), 2, axis=1), jnp.repeat(jnp.sin(angles), 2, axis=1))


def rotate(values, cos_table, sin_table):
    pairs = values.reshape(values.shape[:-1] + (HEAD // 2, 2))
    turned = jnp.stack([-pairs[..., 1], pairs[..., 0]], axis=-1).reshape(values.shape)
    return values * cos_table[:, None, :] + turned * sin_table[:, None, :]


def absorb(state, queries, keys, values, lift):
    top, total, weighted = state
    scores = (
        jnp.einsum("qkgd,skd->kgqs", queries, keys, preferred_element_type=jnp.float32)
        * HEAD ** (-0.5)
        + lift
    )
    new_top = jnp.maximum(top, jnp.max(scores, axis=-1))
    factor = jnp.exp(top - new_top)
    weights = jnp.exp(scores - new_top[..., None])
    total = total * factor + jnp.sum(weights, axis=-1)
    weighted = weighted * factor[..., None] + jnp.einsum(
        "kgqs,skd->kgqd", weights.astype(jnp.bfloat16), values, preferred_element_type=jnp.float32
    )
    return (new_top, total, weighted)


def shards(
    latent,
    context,
    conditioning,
    context_conditioning,
    shift_weight,
    scale_weight,
    gate_weight,
    norm_gain,
    query_weight,
    key_weight,
    value_weight,
    query_gain,
    key_gain,
    context_lift,
    output_weight,
):
    key_heads = key_weight.shape[1] // HEAD
    query_heads = query_weight.shape[1] // HEAD
    group = query_heads // key_heads
    key_width = key_heads * HEAD
    query_width = query_heads * HEAD
    signals = jnp.stack([jax.nn.silu(conditioning), jax.nn.silu(context_conditioning)]).astype(
        jnp.bfloat16
    )
    partial_terms = jnp.stack(
        [
            jnp.dot(signals, shift_weight, preferred_element_type=jnp.float32),
            jnp.dot(signals, scale_weight, preferred_element_type=jnp.float32),
            jnp.dot(signals, gate_weight, preferred_element_type=jnp.float32),
        ],
        axis=1,
    )
    summed = lax.psum(partial_terms, "sp")
    modulation = lax.all_gather(summed, "tp", axis=2, tiled=True)
    hidden = (
        normalize(latent.astype(jnp.float32), norm_gain) * (1.0 + modulation[0, 1])
        + modulation[0, 0]
    ).astype(jnp.bfloat16)
    piece = lax.all_gather(hidden, "tp", axis=0, tiled=True)
    projected = jnp.concatenate(
        [
            jnp.dot(piece, query_weight, preferred_element_type=jnp.float32),
            jnp.dot(piece, key_weight, preferred_element_type=jnp.float32),
            jnp.dot(piece, value_weight, preferred_element_type=jnp.float32),
        ],
        axis=1,
    )
    length = projected.shape[0]
    cos_table, sin_table = rotary_tables(lax.axis_index("sp") * length, length)
    queries = rotate(
        normalize(projected[:, :query_width].reshape(length, query_heads, HEAD), query_gain),
        cos_table,
        sin_table,
    )
    queries = queries.astype(jnp.bfloat16).reshape(length, key_heads, group, HEAD)
    keys = rotate(
        normalize(
            projected[:, query_width : query_width + key_width].reshape(length, key_heads, HEAD),
            key_gain,
        ),
        cos_table,
        sin_table,
    )
    values = projected[:, query_width + key_width :].astype(jnp.bfloat16)
    packed = jnp.concatenate([keys.astype(jnp.bfloat16).reshape(length, key_width), values], axis=1)
    context_hidden = (
        normalize(context.astype(jnp.float32), norm_gain) * (1.0 + modulation[1, 1])
        + modulation[1, 0]
    ).astype(jnp.bfloat16)
    context_count = context.shape[0]
    context_keys = normalize(
        jnp.dot(context_hidden, key_weight, preferred_element_type=jnp.float32).reshape(
            context_count, key_heads, HEAD
        ),
        key_gain,
    )
    context_values = jnp.dot(
        context_hidden, value_weight, preferred_element_type=jnp.float32
    ).astype(jnp.bfloat16)
    context_packed = lax.all_gather(
        jnp.concatenate(
            [context_keys.astype(jnp.bfloat16).reshape(context_count, key_width), context_values],
            axis=1,
        ),
        "sp",
        axis=0,
        tiled=True,
    )
    context_total = context_packed.shape[0]
    start_state = (
        jnp.full((key_heads, group, length), -jnp.inf, jnp.float32),
        jnp.zeros((key_heads, group, length), jnp.float32),
        jnp.zeros((key_heads, group, length, HEAD), jnp.float32),
    )
    lift = context_lift.reshape(key_heads, group, 1, 1)
    state = absorb(
        start_state,
        queries,
        context_packed[:, :key_width].reshape(context_total, key_heads, HEAD),
        context_packed[:, key_width:].reshape(context_total, key_heads, HEAD),
        lift,
    )
    piece = lax.all_gather(packed, "sp", axis=0, tiled=True)
    count = piece.shape[0]
    block = math.gcd(count, 2048)

    def one_block(index, inner):
        part = lax.dynamic_slice_in_dim(piece, index * block, block, 0)
        return absorb(
            inner,
            queries,
            part[:, :key_width].reshape(block, key_heads, HEAD),
            part[:, key_width:].reshape(block, key_heads, HEAD),
            0.0,
        )

    top, total, weighted = lax.fori_loop(0, count // block, one_block, state)
    attended = weighted / total[..., None]
    attended = (
        jnp.transpose(attended, (2, 0, 1, 3)).reshape(length, query_width).astype(jnp.bfloat16)
    )
    by_rows = lax.all_to_all(attended, "tp", split_axis=0, concat_axis=1, tiled=True)
    projection = jnp.dot(
        by_rows,
        lax.all_gather(output_weight, "tp", axis=0, tiled=True),
        preferred_element_type=jnp.float32,
    )
    return (latent.astype(jnp.float32) + modulation[0, 2] * projection).astype(jnp.bfloat16)


def solution(mesh):
    in_specs = (
        P(("sp", "tp"), None),
        P("sp", None),
        P("sp"),
        P("sp"),
        P("sp", "tp"),
        P("sp", "tp"),
        P("sp", "tp"),
        P(),
        P(None, "tp"),
        P(None, "tp"),
        P(None, "tp"),
        P(),
        P(),
        P("tp"),
        P("tp", None),
    )
    out_specs = P(("sp", "tp"), None)
    return jax.shard_map(shards, mesh=mesh, in_specs=in_specs, out_specs=out_specs, check_vma=False)
```

profile of v0, /device:TPU:0, one launch (start us, length us, event | category | flops | bytes accessed | tf_op | source)
XLA Modules:
  0.0 280.8 jit_solution(9180749674133689789)
XLA Ops:
  6.5 0.8 fusion.43
  7.4 0.7 fusion.44
  8.1 1.1 convolution_bitcast_fusion
  9.2 1.1 convolution_bitcast_fusion.1
  10.3 1.1 convolution_bitcast_fusion.2
  11.4 38.8 %psum.7 = f32[2,3,512]{2,0,1:T(2,128)S(1)} all-reduce(f32[2,3,512]{2,0,1:T(2,128)S(1)} %pad_maximum_fusion.5), channel_id=1, replica_groups=mesh['sp'=8,'tp'=4] {'sp'}, use_global_device_ids=true, to_apply=%region_0.1 | all-reduce | flops 3072 | bytes 24576 | tf_op jit(solution)/shard_map/psum | solution.py:85
  50.2 5.2 %all_gather.15 = f32[2,3,2048]{2,0,1:T(2,128)S(1)} all-gather(f32[2,3,512]{2,0,1:T(2,128)S(1)} %psum.7), channel_id=1, replica_groups=mesh['sp'=8,'tp'=4] {'tp'}, dimensions={2}, use_global_device_ids=true | all-gather | bytes 61440 | tf_op jit(solution)/shard_map/all_gather | solution.py:86
  55.4 0.6 fusion.49
  56.1 1.2 fusion.19
  57.3 2.1 fusion.23
  59.6 0.2 fusion.34
  59.9 0.1 mul.343
  60.1 0.1 mul.351
  60.2 0.8 mul.369
  60.9 0.7 mul.320
  61.7 17.7 %all-gather.4.cloned.1.call-done = bf16[512,2048]{1,0:T(8,128)(2,1)} async-done(((bf16[128,2048]{1,0:T(8,128)(2,1)}), bf16[512,2048]{1,0:T(8,128)(2,1)}) %all-gather.4.cloned.1.call-update) | async-done | bytes 2097168 | tf_op jit(solution)/shard_map/all_gather | solution.py:91
  79.4 2.6 bitcast_reduce_fusion.3
  82.1 0.3 reshape.187
  82.4 0.3 multiply_multiply_fusion.1
  82.7 0.4 slice_negate_fusion.1
  83.1 0.5 pad_maximum_fusion.1
  83.6 1.2 reshape.188
  84.7 1.2 fusion.30
  86.0 2.6 convolution_convert_fusion
  88.6 0.8 pad_maximum_fusion.2
  89.5 0.7 all-gather.8.cloned.1.call-update
  90.2 0.2 fusion.24
  90.4 1.6 fusion.50
  92.0 1.6 convolution_convert_fusion.1
  93.5 0.7 mul.348
  94.3 0.1 mul.316
  94.4 0.1 reduce_sum.68
  94.5 0.1 mul.317
  94.7 0.1 mul.318
  94.8 32.9 %all_gather.16 = bf16[512,512]{1,0:T(8,128)(2,1)S(1)} all-gather(bf16[64,512]{1,0:T(8,128)(2,1)S(1)} %pad_maximum_fusion.3), channel_id=1, replica_groups=mesh['sp'=8,'tp'=4] {'sp'}, dimensions={0}, use_global_device_ids=true | all-gather | bytes 589824 | tf_op jit(solution)/shard_map/all_gather | solution.py:132
  127.8 0.1 copy.43
  127.9 1.3 add.225
  129.3 0.8 copy.44
  130.1 3.6 %bitcast_reduce_fusion.2 = (f32[512,8]{0,1:T(8,128)}, f32[512,512]{0,1:T(8,128)S(1)}) fusion(bf16[512,2048]{1,0:T(8,128)(2,1)} %all-gather.4.cloned.1.call-done, bf16[2048,512]{1,0:T(8,128)(2,1)S(1)} %copy-done), kind=kOutput, calls=%fused_computation.35 | convolution fusion | flops 1074262016 | bytes 5259264 | tf_op jit(solution)/shard_map/dot_general | solution.py:94
  133.7 0.6 reshape.184
  134.3 0.7 add_rsqrt_fusion.1
  135.0 0.6 rsqrt.48
  135.7 1.2 multiply_multiply_fusion
  136.8 0.9 slice_negate_fusion
  137.7 1.9 pad_maximum_fusion
  139.6 2.0 reshape.185
  141.6 1.3 add_convert_fusion
  142.9 2.2 bitcast_reduce_fusion.1
  145.1 1.7 fusion.11
  146.9 2.4 fusion.16
  149.3 20.4 %all-gather.6.cloned.1.call-done = bf16[4096,512]{0,1:T(8,128)(2,1)} async-done(((bf16[512,512]{0,1:T(8,128)(2,1)}), bf16[4096,512]{0,1:T(8,128)(2,1)}) %all-gather.6.cloned.1.call-update) | async-done | bytes 4194320 | tf_op jit(solution)/shard_map/all_gather | solution.py:155
  169.7 87.2 %while.17 = (s32[]{:T(128)}, f32[4,2,512]{2,1,0:T(2,128)S(1)}, f32[4,2,512]{2,1,0:T(2,128)S(1)}, f32[4,2,512,64]{2,3,1,0:T(8,128)S(1)}, bf16[4096,512]{0,1:T(8,1...) while((s32[]{:T(128)}, f32[4,2,512]{2,1,0:T(2,128)S(1)}, ...), condition=%wide.region_11.12_spmd, body=%wide.region_8.11_spmd.sunk | while | flops 2215124992 | bytes 109838512 | solution.py:169
  169.7 1.8 fusion.81
  171.5 15.8 %bitcast_reduce_fusion.5 = (f32[4,2,512]{2,1,0:T(2,128)S(1)}, f32[4,2048,512,2]{2,1,3,0:T(8,128)}) fusion(bf16[2048,4,64,1]{0,2,3,1:T(8,128)(2,1)S(1)} %bitcast.152, bf16[512,4,2,64]{0,3,2,1:T(8,128)(2,1)S(1)} %get-tuple-element.242), kind=kOutput, calls=%fused_computation.1.clone.1 | convolution fusion | flops 1090514944 | bytes 35143680 | tf_op jit(solution)/shard_map/while/body/eval_jaxpr/qkgd,skd->kgqs/dot_general | solution.py:38
  187.3 13.7 %fusion.82 = f32[4,2,512]{2,1,0:T(2,128)S(1)} fusion(f32[4,2048,512,2]{2,1,3,0:T(8,128)} %get-tuple-element.211, f32[4,2,512]{2,1,0:T(2,128)S(1)} %max.8), kind=kLoop, calls=%fused_computation.4.clone.1 | loop fusion | flops 25161728 | bytes 33587200 | tf_op jit(solution)/shard_map/while/body/eval_jaxpr/reduce_sum | solution.py:45
  201.1 13.7 %fusion.83 = f32[4,2,512,64]{2,3,1,0:T(8,128)S(1)} fusion(bf16[2048,4,64,1]{0,2,3,1:T(8,128)(2,1)S(1)} %bitcast.153, f32[4,2048,512,2]{2,1,3,0:T(8,128)} %get-tuple-element.211, f32[4,2,512]{2,1,0:T(2,128)S(1)} %max.8, f32[4,2,512,64]{2,3,1,0:T(8,128)S(1)} %get-tuple-element.229, f32[4,2,512]{2,1,0:T(2,128)S(1)} %bitcast.159), kind=kOutput, calls=%fused_computation.6.clone.1 | convolution fusion | flops 1099431936 | bytes 36732928 | tf_op jit(solution)/shard_map/while/body/eval_jaxpr/kgqs,skd->kgqd/dot_general | solution.py:46
  214.8 1.7 fusion.81
  216.5 13.3 %bitcast_reduce_fusion.5 = (f32[4,2,512]{2,1,0:T(2,128)S(1)}, f32[4,2048,512,2]{2,1,3,0:T(8,128)}) fusion(bf16[2048,4,64,1]{0,2,3,1:T(8,128)(2,1)S(1)} %bitcast.152, bf16[512,4,2,64]{0,3,2,1:T(8,128)(2,1)S(1)} %get-tuple-element.242), kind=kOutput, calls=%fused_computation.1.clone.1 | convolution fusion | flops 1090514944 | bytes 35143680 | tf_op jit(solution)/shard_map/while/body/eval_jaxpr/qkgd,skd->kgqs/dot_general | solution.py:38
  229.8 13.6 %fusion.82 = f32[4,2,512]{2,1,0:T(2,128)S(1)} fusion(f32[4,2048,512,2]{2,1,3,0:T(8,128)} %get-tuple-element.211, f32[4,2,512]{2,1,0:T(2,128)S(1)} %max.8), kind=kLoop, calls=%fused_computation.4.clone.1 | loop fusion | flops 25161728 | bytes 33587200 | tf_op jit(solution)/shard_map/while/body/eval_jaxpr/reduce_sum | solution.py:45
  243.4 13.5 %fusion.83 = f32[4,2,512,64]{2,3,1,0:T(8,128)S(1)} fusion(bf16[2048,4,64,1]{0,2,3,1:T(8,128)(2,1)S(1)} %bitcast.153, f32[4,2048,512,2]{2,1,3,0:T(8,128)} %get-tuple-element.211, f32[4,2,512]{2,1,0:T(2,128)S(1)} %max.8, f32[4,2,512,64]{2,3,1,0:T(8,128)S(1)} %get-tuple-element.229, f32[4,2,512]{2,1,0:T(2,128)S(1)} %bitcast.159), kind=kOutput, calls=%fused_computation.6.clone.1 | convolution fusion | flops 1099431936 | bytes 36732928 | tf_op jit(solution)/shard_map/while/body/eval_jaxpr/kgqs,skd->kgqd/dot_general | solution.py:46
  256.9 0.1 fusion.32
  257.1 0.1 convert_element_type.83
  257.3 11.5 %all_to_all.16 = bf16[4,128,512]{1,2,0:T(8,128)(2,1)S(1)} all-to-all(bf16[4,128,512]{1,2,0:T(8,128)(2,1)S(1)} %copy.46), channel_id=1, replica_groups=mesh['sp'=8,'tp'=4] {'tp'}, dimensions={0} | all-to-all | bytes 1048576 | tf_op jit(solution)/shard_map/all_to_all | solution.py:174
  268.8 5.5 %fusion.15 = bf16[128,2048]{1,0:T(8,128)(2,1)} fusion(bf16[128,2048]{0,1:T(8,128)(2,1)S(1)} %bitcast.156, bf16[2048,2048]{1,0:T(8,128)(2,1)} %all-gather.8.cloned.1.call-done, bf16[128,2048]{1,0:T(8,128)(2,1)S(1)} %copy-done.2, f32[2048]{0:T(1024)S(1)} %bitcast.164), kind=kOutput, calls=%fused_computation.20 | convolution fusion | flops 1074790400 | bytes 9969664 | tf_op jit(solution)/shard_map/dot_general | solution.py:175
  (50 shorter events, 0.7 us)
Async XLA Ops:
  6.5 123.6 %copy-start = (bf16[2048,512]{1,0:T(8,128)(2,1)S(1)}, bf16[2048,512]{1,0:T(8,128)(2,1)}, u32[]{:S(2)}) copy-start(bf16[2048,512]{1,0:T(8,128)(2,1)} %param.25) | copy-start | bytes 6291460
  6.5 72.9 %all-gather.4.cloned.1.call-start = ((), (), s32[]{:S(2)}) async-start(), calls=%async_computation.1 | async-start | bytes 2621440 | tf_op jit(solution)/shard_map/all_gather | solution.py:91
  59.4 110.3 %all-gather.6.cloned.1.call-start = ((), (), s32[]{:S(2)}) async-start(), calls=%async_computation.2 | async-start | bytes 4718592 | tf_op jit(solution)/shard_map/all_gather | solution.py:155
  60.2 30.0 %copy-start.3 = (f32[512,64]{0,1:T(8,128)}, f32[512,64]{0,1:T(8,128)S(1)}, u32[]{:S(2)}) copy-start(f32[512,64]{0,1:T(8,128)S(1)} %mul.351) | copy-start | bytes 393220
  61.7 28.7 %copy-start.7 = (f32[2048]{0:T(1024)S(1)}, f32[2048]{0:T(1024)}, u32[]{:S(2)}) copy-start(f32[2048]{0:T(1024)} %param.24) | copy-start | bytes 24580
  82.4 11.1 %copy-start.9 = (f32[64]{0:T(128)S(1)}, f32[64]{0:T(128)}, u32[]{:S(2)}) copy-start(f32[64]{0:T(128)} %param.28) | copy-start | bytes 772
  84.7 5.5 %copy-start.4 = (bf16[64,2048]{1,0:T(8,128)(2,1)S(1)}, bf16[64,2048]{1,0:T(8,128)(2,1)}, u32[]{:S(2)}) copy-start(bf16[64,2048]{1,0:T(8,128)(2,1)} %param.18) | copy-start | bytes 786436
  89.5 179.3 %all-gather.8.cloned.1.call-start = ((), (), s32[]{:S(2)}) async-start(), calls=%async_computation.3 | async-start | bytes 10485760 | tf_op jit(solution)/shard_map/all_gather | solution.py:177
  141.6 3.5 %copy-start.6 = (f32[4,2]{1,0:T(4,128)S(1)}, f32[4,2]{1,0:T(4,128)}, u32[]{:S(2)}) copy-start(f32[4,2]{1,0:T(4,128)} %add.225) | copy-start | bytes 100
  142.9 4.0 %copy-start.5 = (bf16[512,256]{0,1:T(8,128)(2,1)S(1)}, bf16[512,256]{0,1:T(8,128)(2,1)}, u32[]{:S(2)}) copy-start(bf16[512,256]{0,1:T(8,128)(2,1)} %copy.44) | copy-start | bytes 786436
  169.7 99.1 %copy-start.2 = (bf16[128,2048]{1,0:T(8,128)(2,1)S(1)}, bf16[128,2048]{1,0:T(8,128)(2,1)}, u32[]{:S(2)}) copy-start(bf16[128,2048]{1,0:T(8,128)(2,1)} %param.17) | copy-start | bytes 1572868
  169.7 99.1 %copy-start.8 = (f32[1,1,2048]{2,0,1:T(1,128)S(1)}, f32[1,1,2048]{2,0,1:T(1,128)}, u32[]{:S(2)}) copy-start(f32[1,1,2048]{2,0,1:T(1,128)} %get-tuple-element.143) | copy-start | bytes 24580
  257.3 17.0 %copy-start.1 = (bf16[2048,512]{1,0:T(8,128)(2,1)S(1)}, bf16[2048,512]{1,0:T(8,128)(2,1)}, u32[]{:S(2)}) copy-start(bf16[2048,512]{1,0:T(8,128)(2,1)} %param.25) | copy-start | bytes 6291460
Sparse Core Ops, SparseCore 0:
  59.6 19.8 all-gather.3
  89.6 80.0 all-gather.5
  171.3 56.4 all-gather.7
where the time goes:
time: 282 us; the launch traced here: 281 us
  blocking collectives  88.5 us (31%)
  matrix products  81.5 us (29%)
  other arithmetic  44.6 us (16%)
  waiting for transfers between devices  38.9 us (14%)
  local copies, waits for them, and re-layouts  13.6 us (5%)
  between operations  13.5 us (5%)
    psum x1, blocking collectives, shards(): summed = lax.psum(partial_terms, 'sp')  38.8 us
    all_gather x1, blocking collectives, shards(): lax.all_gather(jnp.concatenate([context_keys.astype(jnp.bfloat16).reshape...  32.9 us
    dot_general x3, matrix products, absorb(): jnp.einsum('qkgd,skd->kgqs', queries, keys, preferred_element_type=jnp.fl...  31.3 us
    dot_general x3, matrix products, absorb(): jnp.einsum('kgqs,skd->kgqd', weights.astype(jnp.bfloat16), values, prefer...  29.6 us
    reduce_sum x3, other arithmetic, absorb(): total = total * factor + jnp.sum(weights, axis=-1)  29 us
    all_gather x1, waiting for transfers between devices, shards(): piece = lax.all_gather(packed, 'sp', axis=0, tiled=True)  20.4 us
    all_gather x1, waiting for transfers between devices, shards(): piece = lax.all_gather(hidden, 'tp', axis=0, tiled=True)  17.7 us
    all_to_all x1, blocking collectives, shards(): lax.all_to_all(attended, 'tp', split_axis=0, concat_axis=1, tiled=True)  11.5 us
  transfers between devices with their start and end apart: 3, of which 2 were waited for; matrix products, arithmetic and copies ran while one was open for 41% of the time, Pallas kernels for 0%

commit v1 on v0

--- a/solution.py
+++ b/solution.py
@@ -88,7 +88,12 @@
         normalize(latent.astype(jnp.float32), norm_gain) * (1.0 + modulation[0, 1])
         + modulation[0, 0]
     ).astype(jnp.bfloat16)
-    piece = lax.all_gather(hidden, "tp", axis=0, tiled=True)
+    ring = [hidden]
+    for hop in range(3):
+        ring.append(lax.ppermute(ring[-1], "tp", [(dev, (dev + 1) % 4) for dev in range(4)]))
+    piece = jnp.roll(
+        jnp.concatenate(ring[::-1], axis=0), (lax.axis_index("tp") + 1) * ring[0].shape[0], axis=0
+    )
     projected = jnp.concatenate(
         [
             jnp.dot(piece, query_weight, preferred_element_type=jnp.float32),

time: 282 us -> 291 us (1.032)
  local copies, waits for them, and re-layouts: 13.6 us -> 20.5 us
    ppermute x0 -> x3, waiting for transfers between devices: none -> 21.6 us  [shards(): lax.ppermute(ring[-1], 'tp', [(dev, (dev + 1) % 4) for dev in range(4)])]
    all_gather x1 -> x0, waiting for transfers between devices: 17.7 us -> none  [shards(): piece = lax.all_gather(hidden, 'tp', axis=0, tiled=True)]
    unnamed x20 -> x44, local copies, waits for them, and re-layouts: 0.04 us -> 6.12 us
  transfers between devices with their start and end apart: 3 -> 5, of which waited for: 2 -> 4; matrix products, arithmetic and copies ran while one was open for 41% -> 40% of each run, Pallas kernels for 0% -> 0%
where the time goes in v1:
time: 291 us; the launch traced here: 290 us
  blocking collectives  88.6 us (30%)
  matrix products  79.7 us (27%)
  other arithmetic  46.7 us (16%)
  waiting for transfers between devices  40.1 us (14%)
  local copies, waits for them, and re-layouts  20.5 us (7%)
  between operations  13.9 us (5%)
    psum x1, blocking collectives, shards(): summed = lax.psum(partial_terms, 'sp')  38.8 us
    all_gather x1, blocking collectives, shards(): lax.all_gather(jnp.concatenate([context_keys.astype(jnp.bfloat16).reshape...  33 us
    dot_general x3, matrix products, absorb(): jnp.einsum('qkgd,skd->kgqs', queries, keys, preferred_element_type=jnp.fl...  31.3 us
    dot_general x3, matrix products, absorb(): jnp.einsum('kgqs,skd->kgqd', weights.astype(jnp.bfloat16), values, prefer...  29.6 us
    reduce_sum x3, other arithmetic, absorb(): total = total * factor + jnp.sum(weights, axis=-1)  29 us
    ppermute x3, waiting for transfers between devices, shards(): lax.ppermute(ring[-1], 'tp', [(dev, (dev + 1) % 4) for dev in range(4)])  21.6 us
    all_gather x1, waiting for transfers between devices, shards(): piece = lax.all_gather(packed, 'sp', axis=0, tiled=True)  17.8 us
    all_to_all x1, blocking collectives, shards(): lax.all_to_all(attended, 'tp', split_axis=0, concat_axis=1, tiled=True)  11.5 us
  transfers between devices with their start and end apart: 5, of which 4 were waited for; matrix products, arithmetic and copies ran while one was open for 40% of the time, Pallas kernels for 0%

profile of v1, /device:TPU:0, one launch (start us, length us, event | category | flops | bytes accessed | tf_op | source)
XLA Modules:
  0.0 290.1 jit_solution(8988126137939520881)
XLA Ops:
  6.5 0.8 fusion.52
  7.4 0.7 fusion.53
  8.1 1.1 convolution_bitcast_fusion
  9.2 1.1 convolution_bitcast_fusion.1
  10.3 1.1 convolution_bitcast_fusion.2
  11.4 38.8 %psum.7 = f32[2,3,512]{2,0,1:T(2,128)S(1)} all-reduce(f32[2,3,512]{2,0,1:T(2,128)S(1)} %pad_maximum_fusion.5), channel_id=1, replica_groups=mesh['sp'=8,'tp'=4] {'sp'}, use_global_device_ids=true, to_apply=%region_0.1 | all-reduce | flops 3072 | bytes 24576 | tf_op jit(solution)/shard_map/psum | solution.py:85
  50.2 5.2 %all_gather.12 = f32[2,3,2048]{2,0,1:T(2,128)S(1)} all-gather(f32[2,3,512]{2,0,1:T(2,128)S(1)} %psum.7), channel_id=1, replica_groups=mesh['sp'=8,'tp'=4] {'tp'}, dimensions={2}, use_global_device_ids=true | all-gather | bytes 61440 | tf_op jit(solution)/shard_map/all_gather | solution.py:86
  55.4 0.6 fusion.61
  56.1 1.2 fusion.28
  57.3 0.5 copy-done.16
  57.9 1.3 fusion.32
  59.2 0.4 collective-permute-start
  59.6 8.3 %collective-permute-done = bf16[128,2048]{1,0:T(8,128)(2,1)S(1)} collective-permute-done((bf16[128,2048]{1,0:T(8,128)(2,1)S(1)}, bf16[128,2048]{1,0:T(8,128)(2,1)S(1)}, u32[]{:S(2)}, u32[]{:S(2)}) %collective-permute-start) | collective-permute-done | bytes 524320 | tf_op jit(solution)/shard_map/ppermute | solution.py:93
  67.8 1.4 mul.373
  69.2 7.3 %collective-permute-done.1 = bf16[128,2048]{1,0:T(8,128)(2,1)} collective-permute-done((bf16[128,2048]{1,0:T(8,128)(2,1)S(1)}, bf16[128,2048]{1,0:T(8,128)(2,1)}, u32[]{:S(2)}, u32[]{:S(2)}) %collective-permute-start.1) | collective-permute-done | bytes 524320 | tf_op jit(solution)/shard_map/ppermute | solution.py:93
  76.7 0.9 fusion.43
  77.7 0.9 broadcast_in_dim.13
  78.7 0.7 mul.323
  79.5 6.0 %collective-permute-done.2 = bf16[128,2048]{1,0:T(8,128)(2,1)} collective-permute-done((bf16[128,2048]{1,0:T(8,128)(2,1)}, bf16[128,2048]{1,0:T(8,128)(2,1)}, u32[]{:S(2)}, u32[]{:S(2)}) %collective-permute-start.2) | collective-permute-done | bytes 524320 | tf_op jit(solution)/shard_map/ppermute | solution.py:93
  85.5 1.1 constant_dynamic-update-slice_fusion.7
  86.5 1.1 constant_dynamic-update-slice_fusion.6
  87.7 1.4 constant_dynamic-update-slice_fusion.4
  89.0 1.1 constant_dynamic-update-slice_fusion.3
  90.1 1.1 constant_dynamic-update-slice_fusion.2
  91.2 1.0 constant_dynamic-update-slice_fusion
  92.3 0.8 bitcast_reduce_fusion.3
  93.0 1.1 copy-done.12
  94.8 0.4 slice_negate_fusion.1
  95.2 0.5 pad_maximum_fusion.1
  95.7 1.2 reshape.188
  96.9 2.6 fusion.25
  99.5 1.2 fusion.39
  100.7 0.8 pad_maximum_fusion.2
  101.6 0.7 all-gather.5.cloned.1.call-update
  102.5 1.6 fusion.62
  104.1 1.6 convolution_convert_fusion
  105.7 0.7 mul.352
  107.0 33.0 %all_gather.13 = bf16[512,512]{1,0:T(8,128)(2,1)S(1)} all-gather(bf16[64,512]{1,0:T(8,128)(2,1)S(1)} %pad_maximum_fusion.3), channel_id=1, replica_groups=mesh['sp'=8,'tp'=4] {'sp'}, dimensions={0}, use_global_device_ids=true | all-gather | bytes 589824 | tf_op jit(solution)/shard_map/all_gather | solution.py:137
  140.2 0.7 add.241
  140.9 0.9 copy.44
  141.7 3.5 %bitcast_reduce_fusion.2 = (f32[512,8]{0,1:T(8,128)}, f32[512,512]{0,1:T(8,128)S(1)}) fusion(bf16[2048,512]{1,0:T(8,128)(2,1)S(1)} %copy-done, bf16[1024,2048]{1,0:T(8,128)(2,1)} %copy-done.12, s32[]{:T(128)S(6)} %select_n.40), kind=kOutput, calls=%fused_computation.41 | convolution fusion | flops 1074262016 | bytes 5259268 | tf_op jit(solution)/shard_map/dot_general | solution.py:99
  145.3 0.6 reshape.184
  145.9 0.7 add_rsqrt_fusion.1
  146.6 0.6 rsqrt.48
  147.2 1.2 multiply_multiply_fusion
  148.4 0.9 slice_negate_fusion
  149.3 1.9 pad_maximum_fusion
  151.2 1.9 reshape.185
  153.2 1.3 add_convert_fusion
  154.5 2.2 bitcast_reduce_fusion.1
  156.7 1.7 fusion.11
  158.5 2.4 fusion.22
  160.8 17.8 %all-gather.3.cloned.1.call-done = bf16[4096,512]{0,1:T(8,128)(2,1)} async-done(((bf16[512,512]{0,1:T(8,128)(2,1)}), bf16[4096,512]{0,1:T(8,128)(2,1)}) %all-gather.3.cloned.1.call-update) | async-done | bytes 4194320 | tf_op jit(solution)/shard_map/all_gather | solution.py:160
  178.7 87.2 %while.17 = (s32[]{:T(128)}, f32[4,2,512]{2,1,0:T(2,128)S(1)}, f32[4,2,512]{2,1,0:T(2,128)S(1)}, f32[4,2,512,64]{2,3,1,0:T(8,128)S(1)}, bf16[4096,512]{0,1:T(8,1...) while((s32[]{:T(128)}, f32[4,2,512]{2,1,0:T(2,128)S(1)}, ...), condition=%wide.region_11.12_spmd, body=%wide.region_8.11_spmd.sunk | while | flops 2215124992 | bytes 109838512 | solution.py:174
  178.7 1.8 fusion.90
  180.5 15.8 %bitcast_reduce_fusion.5 = (f32[4,2,512]{2,1,0:T(2,128)S(1)}, f32[4,2048,512,2]{2,1,3,0:T(8,128)}) fusion(bf16[2048,4,64,1]{0,2,3,1:T(8,128)(2,1)S(1)} %bitcast.149, bf16[512,4,2,64]{0,3,2,1:T(8,128)(2,1)S(1)} %get-tuple-element.242), kind=kOutput, calls=%fused_computation.1.clone.1 | convolution fusion | flops 1090514944 | bytes 35143680 | tf_op jit(solution)/shard_map/while/body/eval_jaxpr/qkgd,skd->kgqs/dot_general | solution.py:38
  196.3 13.7 %fusion.91 = f32[4,2,512]{2,1,0:T(2,128)S(1)} fusion(f32[4,2048,512,2]{2,1,3,0:T(8,128)} %get-tuple-element.211, f32[4,2,512]{2,1,0:T(2,128)S(1)} %max.8), kind=kLoop, calls=%fused_computation.4.clone.1 | loop fusion | flops 25161728 | bytes 33587200 | tf_op jit(solution)/shard_map/while/body/eval_jaxpr/reduce_sum | solution.py:45
  210.0 13.7 %fusion.92 = f32[4,2,512,64]{2,3,1,0:T(8,128)S(1)} fusion(bf16[2048,4,64,1]{0,2,3,1:T(8,128)(2,1)S(1)} %bitcast.150, f32[4,2048,512,2]{2,1,3,0:T(8,128)} %get-tuple-element.211, f32[4,2,512]{2,1,0:T(2,128)S(1)} %max.8, f32[4,2,512,64]{2,3,1,0:T(8,128)S(1)} %get-tuple-element.229, f32[4,2,512]{2,1,0:T(2,128)S(1)} %bitcast.156), kind=kOutput, calls=%fused_computation.6.clone.1 | convolution fusion | flops 1099431936 | bytes 36732928 | tf_op jit(solution)/shard_map/while/body/eval_jaxpr/kgqs,skd->kgqd/dot_general | solution.py:46
  223.8 1.7 fusion.90
  225.5 13.3 %bitcast_reduce_fusion.5 = (f32[4,2,512]{2,1,0:T(2,128)S(1)}, f32[4,2048,512,2]{2,1,3,0:T(8,128)}) fusion(bf16[2048,4,64,1]{0,2,3,1:T(8,128)(2,1)S(1)} %bitcast.149, bf16[512,4,2,64]{0,3,2,1:T(8,128)(2,1)S(1)} %get-tuple-element.242), kind=kOutput, calls=%fused_computation.1.clone.1 | convolution fusion | flops 1090514944 | bytes 35143680 | tf_op jit(solution)/shard_map/while/body/eval_jaxpr/qkgd,skd->kgqs/dot_general | solution.py:38
  238.8 13.6 %fusion.91 = f32[4,2,512]{2,1,0:T(2,128)S(1)} fusion(f32[4,2048,512,2]{2,1,3,0:T(8,128)} %get-tuple-element.211, f32[4,2,512]{2,1,0:T(2,128)S(1)} %max.8), kind=kLoop, calls=%fused_computation.4.clone.1 | loop fusion | flops 25161728 | bytes 33587200 | tf_op jit(solution)/shard_map/while/body/eval_jaxpr/reduce_sum | solution.py:45
  252.4 13.5 %fusion.92 = f32[4,2,512,64]{2,3,1,0:T(8,128)S(1)} fusion(bf16[2048,4,64,1]{0,2,3,1:T(8,128)(2,1)S(1)} %bitcast.150, f32[4,2048,512,2]{2,1,3,0:T(8,128)} %get-tuple-element.211, f32[4,2,512]{2,1,0:T(2,128)S(1)} %max.8, f32[4,2,512,64]{2,3,1,0:T(8,128)S(1)} %get-tuple-element.229, f32[4,2,512]{2,1,0:T(2,128)S(1)} %bitcast.156), kind=kOutput, calls=%fused_computation.6.clone.1 | convolution fusion | flops 1099431936 | bytes 36732928 | tf_op jit(solution)/shard_map/while/body/eval_jaxpr/kgqs,skd->kgqd/dot_general | solution.py:46
  266.3 11.5 %all_to_all.16 = bf16[4,128,512]{1,2,0:T(8,128)(2,1)S(1)} all-to-all(bf16[4,128,512]{1,2,0:T(8,128)(2,1)S(1)} %copy.46), channel_id=1, replica_groups=mesh['sp'=8,'tp'=4] {'tp'}, dimensions={0} | all-to-all | bytes 1048576 | tf_op jit(solution)/shard_map/all_to_all | solution.py:179
  277.8 5.5 %fusion.15 = bf16[128,2048]{1,0:T(8,128)(2,1)} fusion(bf16[128,2048]{0,1:T(8,128)(2,1)S(1)} %bitcast.153, bf16[2048,2048]{1,0:T(8,128)(2,1)} %all-gather.5.cloned.1.call-done, bf16[128,2048]{1,0:T(8,128)(2,1)S(1)} %copy-done.3, f32[2048]{0:T(1024)S(1)} %bitcast.167), kind=kOutput, calls=%fused_computation.20 | convolution fusion | flops 1074790400 | bytes 9969664 | tf_op jit(solution)/shard_map/dot_general | solution.py:180
  (79 shorter events, 2.5 us)
Async XLA Ops:
  6.5 135.2 %copy-start = (bf16[2048,512]{1,0:T(8,128)(2,1)S(1)}, bf16[2048,512]{1,0:T(8,128)(2,1)}, u32[]{:S(2)}) copy-start(bf16[2048,512]{1,0:T(8,128)(2,1)} %param.25) | copy-start | bytes 6291460
  6.5 84.7 %copy-start.2 = (bf16[128,2048]{1,0:T(8,128)(2,1)S(1)}, bf16[128,2048]{1,0:T(8,128)(2,1)}, u32[]{:S(2)}) copy-start(bf16[128,2048]{1,0:T(8,128)(2,1)} %param.17) | copy-start | bytes 1572868
  6.5 84.7 %copy-start.8 = (f32[2048]{0:T(1024)S(1)}, f32[2048]{0:T(1024)}, u32[]{:S(2)}) copy-start(f32[2048]{0:T(1024)} %param.24) | copy-start | bytes 24580
  6.5 172.1 %all-gather.3.cloned.1.call-start = ((), (), s32[]{:S(2)}) async-start(), calls=%async_computation.1 | async-start | bytes 4718592 | tf_op jit(solution)/shard_map/all_gather | solution.py:160
  56.1 1.3 copy-start.9
  57.3 0.5 copy-start.16
  59.2 8.7 %collective-permute-start = (bf16[128,2048]{1,0:T(8,128)(2,1)S(1)}, bf16[128,2048]{1,0:T(8,128)(2,1)S(1)}, u32[]{:S(2)}, u32[]{:S(2)}) collective-permute-start(bf16[128,2048]{1,0:T(8,128)(2,1)S(1)} %fusion.32), channel_id=1, source_target_pairs={{0,1},{1,2},{2,3},{3,0},{4,5},{5,6},{6,7},{7,4},{8,9},{9,10},{10,1... | collective-permute-start | bytes 1572872 | tf_op jit(solution)/shard_map/ppermute | solution.py:93
  67.8 8.7 %collective-permute-start.1 = (bf16[128,2048]{1,0:T(8,128)(2,1)S(1)}, bf16[128,2048]{1,0:T(8,128)(2,1)}, u32[]{:S(2)}, u32[]{:S(2)}) collective-permute-start(bf16[128,2048]{1,0:T(8,128)(2,1)S(1)} %collective-permute-done), channel_id=1, source_target_pairs={{0,1},{1,2},{2,3},{3,0},{4,5},{5,6},{6,7},{7,4},{8,9},{9,10},{10,1... | collective-permute-start | bytes 1572872 | tf_op jit(solution)/shard_map/ppermute | solution.py:93
  76.5 8.9 %collective-permute-start.2 = (bf16[128,2048]{1,0:T(8,128)(2,1)}, bf16[128,2048]{1,0:T(8,128)(2,1)}, u32[]{:S(2)}, u32[]{:S(2)}) collective-permute-start(bf16[128,2048]{1,0:T(8,128)(2,1)} %collective-permute-done.1), channel_id=1, source_target_pairs={{0,1},{1,2},{2,3},{3,0},{4,5},{5,6},{6,7},{7,4},{8,9},{9,10},{10,1... | collective-permute-start | bytes 1572872 | tf_op jit(solution)/shard_map/ppermute | solution.py:93
  78.7 20.9 %copy-start.4 = (f32[512,64]{0,1:T(8,128)}, f32[512,64]{0,1:T(8,128)S(1)}, u32[]{:S(2)}) copy-start(f32[512,64]{0,1:T(8,128)S(1)} %mul.355) | copy-start | bytes 393220
  78.7 15.8 %copy-start.11 = (f32[32,2]{1,0:T(8,128)S(1)}, f32[32,2]{1,0:T(8,128)}, u32[]{:S(2)}) copy-start(f32[32,2]{1,0:T(8,128)} %mul.373) | copy-start | bytes 772
  79.5 12.7 %copy-start.5 = (bf16[2048,256]{1,0:T(8,128)(2,1)S(1)}, bf16[2048,256]{1,0:T(8,128)(2,1)}, u32[]{:S(2)}) copy-start(bf16[2048,256]{1,0:T(8,128)(2,1)} %param.26) | copy-start | bytes 3145732
  92.2 1.9 copy-start.12
  92.2 10.3 %copy-start.14 = (f32[1,1,2048]{2,0,1:T(1,128)S(1)}, f32[1,1,2048]{2,0,1:T(1,128)}, u32[]{:S(2)}) copy-start(f32[1,1,2048]{2,0,1:T(1,128)} %get-tuple-element.146) | copy-start | bytes 24580
  92.3 10.3 %copy-start.15 = (f32[1,1,2048]{2,0,1:T(1,128)S(1)}, f32[1,1,2048]{2,0,1:T(1,128)}, u32[]{:S(2)}) copy-start(f32[1,1,2048]{2,0,1:T(1,128)} %get-tuple-element.147) | copy-start | bytes 24580
  94.5 11.2 %copy-start.17 = (f32[64]{0:T(128)S(1)}, f32[64]{0:T(128)}, u32[]{:S(2)}) copy-start(f32[64]{0:T(128)} %param.28) | copy-start | bytes 772
  95.7 44.5 %copy-start.18 = (f32[8]{0:T(128)S(1)}, f32[8]{0:T(128)}, u32[]{:S(2)}) copy-start(f32[8]{0:T(128)} %param.30) | copy-start | bytes 100
  96.9 5.5 %copy-start.6 = (bf16[64,2048]{1,0:T(8,128)(2,1)S(1)}, bf16[64,2048]{1,0:T(8,128)(2,1)}, u32[]{:S(2)}) copy-start(bf16[64,2048]{1,0:T(8,128)(2,1)} %param.18) | copy-start | bytes 786436
  101.6 176.2 %all-gather.5.cloned.1.call-start = ((), (), s32[]{:S(2)}) async-start(), calls=%async_computation.2 | async-start | bytes 10485760 | tf_op jit(solution)/shard_map/all_gather | solution.py:182
  153.2 3.5 %copy-start.10 = (f32[4,2]{1,0:T(4,128)S(1)}, f32[4,2]{1,0:T(4,128)}, u32[]{:S(2)}) copy-start(f32[4,2]{1,0:T(4,128)} %add.241) | copy-start | bytes 100
  154.5 4.0 %copy-start.7 = (bf16[512,256]{0,1:T(8,128)(2,1)S(1)}, bf16[512,256]{0,1:T(8,128)(2,1)}, u32[]{:S(2)}) copy-start(bf16[512,256]{0,1:T(8,128)(2,1)} %copy.44) | copy-start | bytes 786436
  178.7 99.1 %copy-start.3 = (bf16[128,2048]{1,0:T(8,128)(2,1)S(1)}, bf16[128,2048]{1,0:T(8,128)(2,1)}, u32[]{:S(2)}) copy-start(bf16[128,2048]{1,0:T(8,128)(2,1)} %param.17) | copy-start | bytes 1572868
  178.7 99.1 %copy-start.13 = (f32[1,1,2048]{2,0,1:T(1,128)S(1)}, f32[1,1,2048]{2,0,1:T(1,128)}, u32[]{:S(2)}) copy-start(f32[1,1,2048]{2,0,1:T(1,128)} %get-tuple-element.143) | copy-start | bytes 24580
  266.3 17.0 %copy-start.1 = (bf16[2048,512]{1,0:T(8,128)(2,1)S(1)}, bf16[2048,512]{1,0:T(8,128)(2,1)}, u32[]{:S(2)}) copy-start(bf16[2048,512]{1,0:T(8,128)(2,1)} %param.25) | copy-start | bytes 6291460
Sparse Core Ops, SparseCore 0:
  101.7 76.9 all-gather.2
  180.2 56.4 all-gather.4
